TPU v7x, 256 devices: a whole 4x4x8 slice. The times are simulated.
256 devices in a mesh: rep: 2 (over z_hi), fs: 16 (over z_lo, y), tp: 8 (over x, core).
Axes of the slice: x: 4, y: 4, z: 8 (z_hi: 2, z_lo: 4; z = z_hi * 4 + z_lo), core: 2. Of those that a mesh axis runs over, the one named last changes fastest.
Arguments:
- stream: bfloat16 [32, 1024, 2048], P(('rep', 'fs'), None, 'tp'), may hold values from -6 to 6
- norm_gain: float32 [2048], replicated, may hold values from 0.1 to 1.9
- w_in: float32 [2048, 512], P('fs', 'tp'), may hold values from -0.125 to 0.125
- s_in: float32 [512], P(('tp', 'fs')), may hold values from 0.1 to 1.9
- pool_w: bfloat16 [4, 128, 128], replicated, may hold values from -0.5 to 0.5
- w_out: float32 [512, 2048], P('fs', 'tp'), may hold values from -0.25 to 0.25
- s_out: float32 [2048], P(('tp', 'fs')), may hold values from 0.1 to 1.9
- ffn_gain: float32 [2048], replicated, may hold values from 0.1 to 1.9
- w_up: float32 [2048, 8192], P('fs', 'tp'), may hold values from -0.125 to 0.125
- s_up: float32 [8192], P(('tp', 'fs')), may hold values from 0.1 to 1.9
- w_down: float32 [8192, 2048], P('tp', 'fs'), may hold values from -0.0625 to 0.0625
- s_down: float32 [2048], P('fs'), may hold values from 0.1 to 1.9
Outputs:
- result: bfloat16 [32, 1024, 2048], P(('rep', 'fs'), None, 'tp')
All inputs are finite; a program needn't handle non-finite values.
Results may differ from a plain program's by a relative error of at most 0.012.
Values may be sent and summed in bfloat16 or wider, within the bound.
No kernel may reach another device: no remote copies, remote signals or barrier semaphores. Data moves between devices by JAX's collectives and lax.ppermute only.
A program may use at most 64 MiB of HBM per device.

v0:
```python
import jax
import jax.numpy as jnp
from jax import lax
from jax.sharding import Mesh
from jax.sharding import PartitionSpec as P

PW = 512
GROUP = 128
FS = ("fs_0", "fs_1")
REP_FS = ("rep", "fs_0", "fs_1")
TP_FS = ("tp", "fs_0", "fs_1")
epsilon = 0.25


def laid_out(parts, dim):
    parts = jnp.moveaxis(parts, 0, dim)
    lengths = parts.shape
    return parts.reshape(*lengths[:dim], lengths[dim] * lengths[dim + 1], *lengths[dim + 2 :])


def gather_packed(arrays, axis, dims):
    ravelled = jnp.concatenate([a.reshape(-1) for a in arrays])
    lines, at, finished = (lax.all_gather(ravelled, axis), 0, [])
    for a, dim in zip(arrays, dims):
        parts = lines[:, at : at + a.size].reshape(-1, *a.shape)
        finished.append(laid_out(parts, dim))
        at += a.size
    return tuple(finished)


def sent_to_all(array, axis):
    count = lax.axis_size(axis)
    return lax.all_to_all(
        jnp.broadcast_to(array[None], (count, *array.shape)), axis, 0, 0, tiled=True
    )


def collect(array, axis, dim):
    return laid_out(sent_to_all(array, axis), dim)


def stacked_from(array, axes, turns):
    parts = array
    for k in turns:
        parts = lax.all_gather(parts, axes[k])
    done = turns[::-1]
    back = [done.index(k) for k in range(len(axes))]
    parts = parts.transpose(*back, *range(len(axes), parts.ndim))
    return parts.reshape(-1, *array.shape)


def whole_of(array, axes, turns, dim):
    return laid_out(stacked_from(array, axes, turns), dim)


def cut_along(array, dim, count):
    lengths = array.shape
    parts = array.reshape(*lengths[:dim], count, lengths[dim] // count, *lengths[dim + 1 :])
    return jnp.moveaxis(parts, dim, 0)


def sent_and_summed(array, axis, dim):
    count = lax.axis_size(axis)
    parts = lax.all_to_all(cut_along(array, dim, count), axis, 0, 0, tiled=True)
    return jnp.sum(parts.astype(jnp.float32), axis=0)


def rms_rows(values, gain):
    floats = values.astype(jnp.float32)
    scale = lax.rsqrt(jnp.mean(floats * floats, axis=-1, keepdims=True) + epsilon)
    return (floats * scale * gain).astype(jnp.bfloat16)


def pool_local(pool_in, first):
    length, width = pool_in.shape
    positions = jnp.arange(length, dtype=jnp.int32)
    source = positions[None, :]
    target = positions[:, None]
    group_of = (first + jnp.arange(width, dtype=jnp.int32)) // GROUP
    means = jnp.zeros((length, width), jnp.float32)
    for level in range(4):
        half = 2**level
        band_ones = ((source >= target - half) & (source < target + half)).astype(jnp.bfloat16)
        counts = (jnp.minimum(positions + half, length) - jnp.maximum(positions - half, 0)).astype(
            jnp.float32
        )
        sums = jnp.dot(band_ones, pool_in, preferred_element_type=jnp.float32) / counts[:, None]
        means = jnp.where(group_of[None, :] == level, sums, means)
    return (means - pool_in.astype(jnp.float32)).astype(jnp.bfloat16)


def fold_rows(left, piece):
    return jnp.dot(left, piece, preferred_element_type=jnp.float32)


def on_device(
    stream, norm_gain, w_in, s_in, pool_w, w_out, s_out, ffn_gain, w_up, s_up, w_down, s_down
):
    tokens = stream[0]
    length = tokens.shape[0]
    scale_in, scale_out, scale_up, scale_down = gather_packed(
        (s_in, s_out, s_up, s_down), FS, (0, 0, 0, 0)
    )
    in_whole, out_whole = gather_packed(
        (w_in.astype(jnp.bfloat16), w_out.astype(jnp.bfloat16)), FS, (0, 0)
    )
    full_rows = lax.all_gather(tokens, "tp", axis=1, tiled=True)
    normed = rms_rows(full_rows, norm_gain)
    projected = jnp.dot(normed, in_whole, preferred_element_type=jnp.float32)
    pool_in = (projected * scale_in).astype(jnp.bfloat16)
    pooled = pool_local(pool_in, lax.axis_index("tp") * pool_in.shape[1])
    pooled_all = collect(pooled, "tp", 1)
    grouped = jnp.einsum(
        "lgc,gcd->lgd",
        pooled_all.reshape(length, 4, GROUP),
        pool_w,
        preferred_element_type=jnp.float32,
    )
    grouped = grouped.reshape(length, PW).astype(jnp.bfloat16)
    branch = jnp.dot(grouped, out_whole, preferred_element_type=jnp.float32)
    mixed = (tokens.astype(jnp.float32) + branch * scale_out).astype(jnp.bfloat16)
    mixed_full = lax.all_gather(mixed, "tp", axis=1, tiled=True)
    ffn_in = rms_rows(mixed_full, ffn_gain)
    upward = fold_rows(ffn_in, whole_of(w_up.astype(jnp.bfloat16), FS, (0, 1), 0))
    hidden = jnp.square(jax.nn.relu(upward * scale_up)).astype(jnp.bfloat16)
    partial_value = jnp.dot(
        hidden,
        whole_of(w_down.astype(jnp.bfloat16), FS, (0, 1), 1),
        preferred_element_type=jnp.float32,
    )
    rounded = lax.optimization_barrier((partial_value * scale_down).astype(jnp.bfloat16))
    summed = sent_and_summed(rounded.astype(jnp.float32).astype(jnp.bfloat16), "tp", 1)
    return (mixed.astype(jnp.float32) + summed).astype(jnp.bfloat16)[None]


def solution(mesh):
    finer = Mesh(
        mesh.devices.reshape(mesh.shape["rep"], 4, 4, mesh.shape["tp"]),
        ("rep", "fs_0", "fs_1", "tp"),
    )
    return jax.shard_map(
        on_device,
        mesh=finer,
        in_specs=(
            P(REP_FS, None, "tp"),
            P(),
            P(FS, "tp"),
            P(TP_FS),
            P(),
            P(FS, "tp"),
            P(TP_FS),
            P(),
            P(FS, "tp"),
            P(TP_FS),
            P("tp", FS),
            P(FS),
        ),
        out_specs=P(REP_FS, None, "tp"),
        check_vma=False,
    )
```

profile of v0, /device:TPU:1, one launch (start us, length us, event | category | flops | bytes accessed | tf_op | source)
XLA Modules:
  0.0 350.2 jit_solution(10267729505535979363)
XLA Ops:
  6.5 0.0 copy-start
  6.5 0.0 all-gather.18.cloned.1.call-start
  6.5 1.8 convert_element_type.116
  8.4 0.0 all-gather.18.cloned.1.call-update
  8.4 0.0 all-gather.22.cloned.1.call-start
  8.4 1.8 convert_element_type.118
  10.2 0.0 all-gather.22.cloned.1.call-update
  10.2 0.0 all-gather.16.cloned.1.call-start
  10.3 0.7 all-gather.16.cloned.1.call-update
  11.0 0.0 all-gather.20.cloned.1.call-start
  11.0 34.7 %all-gather.18.cloned.1.call-done = bf16[512,1024]{1,0:T(8,128)(2,1)} async-done(((bf16[128,1024]{1,0:T(8,128)(2,1)}), bf16[512,1024]{1,0:T(8,128)(2,1)}) %all-gather.18.cloned.1.call-update) | async-done | bytes 1048592 | tf_op jit(solution)/shard_map/all_gather | solution.py:45
  45.7 0.0 all-gather.20.cloned.1.call-update
  45.8 0.0 all-gather.24.cloned.1.call-start
  45.8 0.8 convert_element_type.100
  46.6 0.1 copy.25
  46.7 0.1 reshape.137
  46.8 0.8 convert_bitcast_fusion
  47.6 1.3 dynamic-slice
  49.6 0.9 maximum_dynamic-update-slice_fusion
  50.5 64.0 %all-reduce = f32[3392]{0:T(1024)S(1)} all-reduce(f32[3392]{0:T(1024)S(1)} %maximum_dynamic-update-slice_fusion), channel_id=4, replica_groups=mesh['rep'=2,'fs_0'=4,'fs_1'=4,'tp'=8] {'fs_0','fs_1'}, use_global_device_ids=true, to_apply=%add | all-reduce | flops 3392 | bytes 27136
  114.5 0.1 reshape.144
  114.6 0.1 mul.87
  114.7 33.1 %all-gather.1 = bf16[262144]{0:T(1024)(128)(2,1)S(1)} all-gather(bf16[16384]{0:T(1024)(128)(2,1)S(1)} %pad_maximum_fusion), channel_id=3, replica_groups=mesh['rep'=2,'fs_0'=4,'fs_1'=4,'tp'=8] {'fs_0','fs_1'}, dimensions={0}, use_global_device_ids=true | all-gather | bytes 557056 | tf_op jit(solution)/shard_map/all_gather | solution.py:23
  147.8 0.2 reshape.143
  148.1 0.0 all-gather.22.cloned.1.call-done
  148.1 0.0 all-gather.24.cloned.1.call-update
  148.2 0.5 reshape_reshape.12
  148.8 0.0 all-gather.16.cloned.1.call-done
  148.9 0.0 copy-start.1
  148.9 3.3 fusion.3
  152.2 0.2 copy-done.1
  152.4 1.5 fusion.69
  153.9 1.4 fusion.63
  155.3 1.4 fusion.57
  156.7 1.4 fusion.51
  158.1 0.0 copy-start.3
  158.1 1.4 fusion.72
  159.5 1.1 broadcast_in_dim.54
  160.6 26.7 %all-to-all-start = ((bf16[8,1024,64]{1,2,0:T(8,128)(2,1)}), bf16[8,1024,64]{1,2,0:T(8,128)(2,1)S(1)}, u32[]{:S(2)}, u32[]{:S(2)}) async-start(bf16[8,1024,64]{1,2,0:T(8,128)(2,1)} %broadcast_in_dim.54), calls=%async_computation | async-start | bytes 2097152 | tf_op jit(solution)/shard_map/all_to_all | solution.py:33
  187.3 0.0 all-gather.14.cloned.1.call-start
  187.3 0.1 slice.27
  187.4 0.1 mul.90
  187.5 0.1 reshape_reshape.14
  187.6 14.7 %all-to-all-done = bf16[8,1024,64]{1,2,0:T(8,128)(2,1)S(1)} async-done(((bf16[8,1024,64]{1,2,0:T(8,128)(2,1)}), bf16[8,1024,64]{1,2,0:T(8,128)(2,1)S(1)}, u32[]{:S(2)}, u32[]{:S(2)}) %all-to-all-start) | async-done | bytes 1048608 | tf_op jit(solution)/shard_map/all_to_all | solution.py:33
  202.3 0.0 copy-done
  202.3 0.5 convolution_convert_fusion
  202.8 1.3 fusion.38
  204.1 0.0 all-gather.14.cloned.1.call-update
  204.1 0.1 slice.28
  204.2 0.1 mul.98
  204.2 0.1 slice_bitcast_fusion
  204.3 4.8 %copy.28 = bf16[4,4,128,1024]{3,2,1,0:T(8,128)(2,1)} copy(bf16[4,4,128,1024]{3,2,0,1:T(8,128)(2,1)} %bitcast.61) | data formatting | bytes 8388608 | tf_op jit(solution)/shard_map/transpose | solution.py:48
  209.1 18.8 %all-gather.24.cloned.1.call-done = bf16[16,1024,128]{2,1,0:T(8,128)(2,1)} async-done(((bf16[4,1024,128]{2,1,0:T(8,128)(2,1)}), bf16[16,1024,128]{2,1,0:T(8,128)(2,1)}) %all-gather.24.cloned.1.call-update) | async-done | bytes 4194320 | tf_op jit(solution)/shard_map/all_gather | solution.py:45
  227.9 4.5 %copy.29 = bf16[4,4,1024,128]{3,2,1,0:T(8,128)(2,1)} copy(bf16[4,4,1024,128]{3,2,0,1:T(8,128)(2,1)} %bitcast.62) | data formatting | bytes 8388608 | tf_op jit(solution)/shard_map/transpose | solution.py:48
  232.4 6.4 %copy.30 = bf16[1024,16,128]{0,2,1:T(8,128)(2,1)} copy(bf16[1024,16,128]{2,0,1:T(8,128)(2,1)} %bitcast.59) | data formatting | bytes 8388608 | tf_op jit(solution)/shard_map/transpose | solution.py:16
  238.8 29.7 %all-gather.14.cloned.1.call-done = bf16[1024,2048]{1,0:T(8,128)(2,1)} async-done(((bf16[1024,256]{1,0:T(8,128)(2,1)}), bf16[1024,2048]{1,0:T(8,128)(2,1)}) %all-gather.14.cloned.1.call-update) | async-done | bytes 4194320 | tf_op jit(solution)/shard_map/all_gather | solution.py:122
  268.6 3.1 fusion
  271.6 0.0 copy-done.5
  271.6 14.6 %multiply_convert_fusion = bf16[1024,2048]{1,0:T(8,128)(2,1)} fusion(bf16[1024,2048]{0,1:T(8,128)(2,1)} %bitcast.64, f32[2048]{0:T(1024)S(1)} %slice_bitcast_fusion, f32[1024]{0:T(1024)S(1)} %mul.98, bf16[2048,1024]{1,0:T(8,128)(2,1)} %bitcast.63, bf16[1024,2048]{1,0:T(8,128)(2,1)} %all-gather.14.cloned.1.call-done, f32[2048]{0:T(1024)S(1)} %copy-done.5, ...), kind=kOutput, calls=%fused_computation.11 | convolution fusion | flops 8606711808 | bytes 16801792 | tf_op jit(solution)/shard_map/dot_general | solution.py:126
  286.3 2.5 copy.37
  288.7 52.6 %all_to_all.10 = bf16[8,1024,256]{2,1,0:T(8,128)(2,1)S(1)} all-to-all(bf16[8,1024,256]{2,1,0:T(8,128)(2,1)S(1)} %bitcast.60), channel_id=1, replica_groups=mesh['rep'=2,'fs_0'=4,'fs_1'=4,'tp'=8] {'tp'}, dimensions={0} | all-to-all | bytes 8388608 | tf_op jit(solution)/shard_map/all_to_all | solution.py:64
  341.4 0.6 convert_reduce_fusion
  342.0 0.5 copy-done.2
  342.4 0.9 fusion.79
  (23 shorter events, 0.2 us)
Async XLA Ops:
  6.5 195.7 %copy-start = (bf16[4,128,128]{2,1,0:T(8,128)(2,1)S(1)}, bf16[4,128,128]{2,1,0:T(8,128)(2,1)}, u32[]{:S(2)}) copy-start(bf16[4,128,128]{2,1,0:T(8,128)(2,1)} %param.16) | copy-start | bytes 393220
  6.5 39.2 %all-gather.18.cloned.1.call-start = ((), (), s32[]{:S(2)}) async-start(), calls=%async_computation.4 | async-start | bytes 1310720 | tf_op jit(solution)/shard_map/all_gather | solution.py:45
  8.4 139.7 %all-gather.22.cloned.1.call-start = ((), (), s32[]{:S(2)}) async-start(), calls=%async_computation.6 | async-start | bytes 1310720 | tf_op jit(solution)/shard_map/all_gather | solution.py:45
  10.2 138.6 %all-gather.16.cloned.1.call-start = ((), (), s32[]{:S(2)}) async-start(), calls=%async_computation.3 | async-start | bytes 4718592 | tf_op jit(solution)/shard_map/all_gather | solution.py:107
  11.0 193.4 %all-gather.20.cloned.1.call-start = ((), (), s32[]{:S(2)}) async-start(), calls=%async_computation.5 | async-start | bytes 5242880 | tf_op jit(solution)/shard_map/all_gather | solution.py:45
  45.8 182.1 %all-gather.24.cloned.1.call-start = ((), (), s32[]{:S(2)}) async-start(), calls=%async_computation.7 | async-start | bytes 5242880 | tf_op jit(solution)/shard_map/all_gather | solution.py:45
  147.8 4.3 %copy-start.4 = (f32[2048]{0:T(1024)S(1)}, f32[2048]{0:T(1024)}, u32[]{:S(2)}) copy-start(f32[2048]{0:T(1024)} %param.13) | copy-start | bytes 24580
  148.9 3.5 %copy-start.1 = (bf16[1,1024,2048]{2,1,0:T(8,128)(2,1)S(1)}, bf16[1,1024,2048]{2,1,0:T(8,128)(2,1)}, u32[]{:S(2)}) copy-start(bf16[1,1024,2048]{2,1,0:T(8,128)(2,1)} %all-gather.16.cloned.1.call-done) | copy-start | bytes 12582916
  158.1 44.7 %copy-start.3 = (bf16[1,1024,256]{2,1,0:T(8,128)(2,1)S(1)}, bf16[1,1024,256]{2,1,0:T(8,128)(2,1)}, u32[]{:S(2)}) copy-start(bf16[1,1024,256]{2,1,0:T(8,128)(2,1)} %param.12) | copy-start | bytes 1572868
  160.6 41.7 %all-to-all-start = ((bf16[8,1024,64]{1,2,0:T(8,128)(2,1)}), bf16[8,1024,64]{1,2,0:T(8,128)(2,1)S(1)}, u32[]{:S(2)}, u32[]{:S(2)}) async-start(bf16[8,1024,64]{1,2,0:T(8,128)(2,1)} %broadcast_in_dim.54), calls=%async_computation | async-start | bytes 2097152 | tf_op jit(solution)/shard_map/all_to_all | solution.py:33
  187.3 81.3 %all-gather.14.cloned.1.call-start = ((), (), s32[]{:S(2)}) async-start(), calls=%async_computation.2 | async-start | bytes 4718592 | tf_op jit(solution)/shard_map/all_gather | solution.py:122
  238.8 32.8 %copy-start.5 = (f32[2048]{0:T(1024)S(1)}, f32[2048]{0:T(1024)}, u32[]{:S(2)}) copy-start(f32[2048]{0:T(1024)} %param.19) | copy-start | bytes 24580
  341.4 1.0 copy-start.2
Sparse Core Ops, SparseCore 0:
  9.1 36.5 all-gather.17
  47.5 33.1 all-gather.21
  82.6 37.5 all-gather.15
  121.8 54.8 all-gather.19
  178.4 49.4 all-gather.23
  229.6 38.9 all-gather.13
where the time goes:
time: 351 us; the launch traced here: 350 us
  blocking collectives  150 us (43%)
  waiting for transfers between devices  98.7 us (28%)
  starting transfers between devices  26.9 us (8%)
  matrix products  23.5 us (7%)
  local copies, waits for them, and re-layouts  23.1 us (7%)
  between operations  14.4 us (4%)
  other arithmetic  13.9 us (4%)
    unnamed x1, blocking collectives  64 us
    all_gather x4, waiting for transfers between devices, stacked_from(): parts = lax.all_gather(parts, axes[k])  53.5 us
    all_to_all x1, blocking collectives, sent_and_summed(): parts = lax.all_to_all(cut_along(array, dim, count), axis, 0, 0, tiled=True)  52.6 us
    all_gather x1, blocking collectives, gather_packed(): lines, at, finished = (lax.all_gather(ravelled, axis), 0, [])  33.1 us
    all_gather x1, waiting for transfers between devices, on_device(): mixed_full = lax.all_gather(mixed, 'tp', axis=1, tiled=True)  29.7 us
    all_to_all x1, starting transfers between devices, sent_to_all(): lax.all_to_all(jnp.broadcast_to(array[None], (count, *array.shape)), axis...  26.7 us
    all_to_all x1, waiting for transfers between devices, sent_to_all(): lax.all_to_all(jnp.broadcast_to(array[None], (count, *array.shape)), axis...  14.7 us
    dot_general x1, matrix products, on_device(): jnp.dot(hidden, whole_of(w_down.astype(jnp.bfloat16), FS, (0, 1), 1), pre...  14.6 us
  transfers between devices with their start and end apart: 7, of which 4 were waited for; matrix products, arithmetic and copies ran while one was open for 10% of the time, Pallas kernels for 0%

commit v1 on v0

--- a/solution.py
+++ b/solution.py
@@ -119,7 +119,31 @@
     grouped = grouped.reshape(length, PW).astype(jnp.bfloat16)
     branch = jnp.dot(grouped, out_whole, preferred_element_type=jnp.float32)
     mixed = (tokens.astype(jnp.float32) + branch * scale_out).astype(jnp.bfloat16)
-    mixed_full = lax.all_gather(mixed, "tp", axis=1, tiled=True)
+    step_out = jax.lax.axis_index("tp")
+    y2 = jax.lax.axis_size("tp")
+    part_next, piece_next, wide_out = (y2, step_out, mixed.shape[1])
+    panels = []
+    for no, m in enumerate(mixed.shape):
+        panels.append(m * part_next if no == 1 else m)
+    fresh = jnp.zeros(panels, mixed.dtype)
+    prior = x_now = mixed
+    mixed_full = lax.dynamic_update_slice_in_dim(fresh, mixed, piece_next * wide_out, axis=1)
+    for c in range(1, part_next // 2 + 1):
+        xs_all = []
+        for no in range(part_next):
+            xs_all.append((no, (no + 1) % part_next))
+        prior = jax.lax.ppermute(prior, "tp", xs_all)
+        mixed_full = lax.dynamic_update_slice_in_dim(
+            mixed_full, prior, (piece_next - c) % part_next * wide_out, axis=1
+        )
+        if 2 * c < part_next:
+            all_rows = []
+            for no in range(part_next):
+                all_rows.append((no, (no - 1) % part_next))
+            x_now = jax.lax.ppermute(x_now, "tp", all_rows)
+            mixed_full = lax.dynamic_update_slice_in_dim(
+                mixed_full, x_now, (piece_next + c) % part_next * wide_out, axis=1
+            )
     ffn_in = rms_rows(mixed_full, ffn_gain)
     upward = fold_rows(ffn_in, whole_of(w_up.astype(jnp.bfloat16), FS, (0, 1), 0))
     hidden = jnp.square(jax.nn.relu(upward * scale_up)).astype(jnp.bfloat16)

time: 351 us -> 340 us (0.969)
  waiting for transfers between devices: 98.7 us -> 63.5 us
  starting transfers between devices: 26.9 us -> 36.3 us
  local copies, waits for them, and re-layouts: 23.1 us -> 31.9 us
  blocking collectives: 150 us -> 157 us
    all_gather x1 -> x0, waiting for transfers between devices: 29.7 us -> none  [on_device(): mixed_full = lax.all_gather(mixed, 'tp', axis=1, tiled=True)]
    all_gather x4, waiting for transfers between devices: 53.5 us -> 34.7 us  [stacked_from(): parts = lax.all_gather(parts, axes[k])]
    ppermute x0 -> x7, waiting for transfers between devices: none -> 13.5 us  [the longest x4 11.1 us: on_device(): prior = jax.lax.ppermute(prior, 'tp', xs_all)]
    ppermute x0 -> x7, starting transfers between devices: none -> 9.17 us  [the longest x4 6.11 us: on_device(): prior = jax.lax.ppermute(prior, 'tp', xs_all)]
    all_gather x1, blocking collectives: 33.1 us -> 39.1 us  [gather_packed(): lines, at, finished = (lax.all_gather(ravelled, axis), 0, [])]
    dynamic_update_slice x0 -> x7, local copies, waits for them, and re-layouts: none -> 5.92 us  [the longest x4 3.39 us: on_device(): lax.dynamic_update_slice_in_dim(mixed_full, prior, (piece_next - c) % par...]
    all_to_all x1, blocking collectives: 52.6 us -> 57.6 us  [sent_and_summed(): parts = lax.all_to_all(cut_along(array, dim, count), axis, 0, 0, tiled=True)]
  transfers between devices with their start and end apart: 7 -> 13, of which waited for: 4 -> 6; matrix products, arithmetic and copies ran while one was open for 10% -> 13% of each run, Pallas kernels for 0% -> 0%
where the time goes in v1:
time: 340 us; the launch traced here: 339 us
  blocking collectives  157 us (46%)
  waiting for transfers between devices  63.5 us (19%)
  starting transfers between devices  36.3 us (11%)
  local copies, waits for them, and re-layouts  31.9 us (9%)
  matrix products  23.5 us (7%)
  between operations  14.1 us (4%)
  other arithmetic  12.6 us (4%)
    unnamed x1, blocking collectives  60.6 us
    all_to_all x1, blocking collectives, sent_and_summed(): parts = lax.all_to_all(cut_along(array, dim, count), axis, 0, 0, tiled=True)  57.6 us
    all_gather x1, blocking collectives, gather_packed(): lines, at, finished = (lax.all_gather(ravelled, axis), 0, [])  39.1 us
    all_gather x4, waiting for transfers between devices, stacked_from(): parts = lax.all_gather(parts, axes[k])  34.7 us
    all_to_all x1, starting transfers between devices, sent_to_all(): lax.all_to_all(jnp.broadcast_to(array[None], (count, *array.shape)), axis...  27 us
    dot_general x1, matrix products, on_device(): jnp.dot(hidden, whole_of(w_down.astype(jnp.bfloat16), FS, (0, 1), 1), pre...  14.7 us
    all_to_all x1, waiting for transfers between devices, sent_to_all(): lax.all_to_all(jnp.broadcast_to(array[None], (count, *array.shape)), axis...  14.5 us
    ppermute x4, waiting for transfers between devices, on_device(): prior = jax.lax.ppermute(prior, 'tp', xs_all)  11.1 us
  transfers between devices with their start and end apart: 13, of which 6 were waited for; matrix products, arithmetic and copies ran while one was open for 13% of the time, Pallas kernels for 0%

profile of v1, /device:TPU:1, one launch (start us, length us, event | category | flops | bytes accessed | tf_op | source)
XLA Modules:
  0.0 339.3 jit_solution(11022188930587272060)
XLA Ops:
  6.6 1.8 convert_element_type.118
  8.4 0.0 all-gather.15.cloned.1.call-start
  8.5 1.8 convert_element_type.116
  10.4 0.7 all-gather.13.cloned.1.call-update
  11.1 34.7 %all-gather.19.cloned.1.call-done = bf16[4096,128]{1,0:T(8,128)(2,1)} async-done(((bf16[1024,128]{1,0:T(8,128)(2,1)}), bf16[4096,128]{1,0:T(8,128)(2,1)}) %all-gather.19.cloned.1.call-update) | async-done | bytes 1048592 | tf_op jit(solution)/shard_map/all_gather | solution.py:45
  45.8 0.8 convert_element_type.100
  46.6 0.1 copy.32
  46.7 0.1 reshape.137
  46.8 0.8 convert_bitcast_fusion
  47.6 39.1 %all-gather.1 = bf16[262144]{0:T(1024)(128)(2,1)S(1)} all-gather(bf16[16384]{0:T(1024)(128)(2,1)S(1)} %pad_maximum_fusion), channel_id=3, replica_groups=mesh['rep'=2,'fs_0'=4,'fs_1'=4,'tp'=8] {'fs_0','fs_1'}, dimensions={0}, use_global_device_ids=true | all-gather | bytes 557056 | tf_op jit(solution)/shard_map/all_gather | solution.py:23
  86.8 0.2 reshape.143
  87.1 0.6 dynamic-slice
  88.4 0.2 maximum_dynamic-update-slice_fusion
  88.6 60.6 %all-reduce = f32[3392]{0:T(1024)S(1)} all-reduce(f32[3392]{0:T(1024)S(1)} %maximum_dynamic-update-slice_fusion), channel_id=4, replica_groups=mesh['rep'=2,'fs_0'=4,'fs_1'=4,'tp'=8] {'fs_0','fs_1'}, use_global_device_ids=true, to_apply=%add | all-reduce | flops 3392 | bytes 27136
  149.2 0.1 reshape.144
  149.3 0.1 mul.111
  149.4 0.5 reshape_reshape.12
  150.1 3.3 fusion.3
  153.4 0.2 copy-done.1
  153.7 1.5 fusion.69
  155.1 1.4 fusion.63
  156.5 1.4 fusion.57
  157.9 1.4 fusion.51
  159.3 1.4 fusion.72
  160.7 1.1 broadcast_in_dim.57
  161.9 27.0 %all-to-all-start = ((bf16[8,1024,64]{1,2,0:T(8,128)(2,1)}), bf16[8,1024,64]{1,2,0:T(8,128)(2,1)S(1)}, u32[]{:S(2)}, u32[]{:S(2)}) async-start(bf16[8,1024,64]{1,2,0:T(8,128)(2,1)} %broadcast_in_dim.57), calls=%async_computation | async-start | bytes 2097152 | tf_op jit(solution)/shard_map/all_to_all | solution.py:33
  188.8 0.1 slice.27
  188.9 0.2 copy.31
  189.1 0.1 mul.114
  189.2 0.1 reshape_reshape.14
  189.3 14.5 %all-to-all-done = bf16[8,1024,64]{1,2,0:T(8,128)(2,1)S(1)} async-done(((bf16[8,1024,64]{1,2,0:T(8,128)(2,1)}), bf16[8,1024,64]{1,2,0:T(8,128)(2,1)S(1)}, u32[]{:S(2)}, u32[]{:S(2)}) %all-to-all-start) | async-done | bytes 1048608 | tf_op jit(solution)/shard_map/all_to_all | solution.py:33
  203.8 0.5 convolution_convert_fusion
  204.3 2.5 broadcast_in_dim.58
  206.8 1.3 constant_dynamic-update-slice_fusion.7
  208.1 1.1 collective-permute-start
  209.2 6.1 %collective-permute-done = bf16[1024,256]{0,1:T(8,128)(2,1)S(1)} collective-permute-done((bf16[1024,256]{0,1:T(8,128)(2,1)S(1)}, bf16[1024,256]{0,1:T(8,128)(2,1)S(1)}, u32[]{:S(2)}, u32[]{:S(2)}) %collective-permute-start) | collective-permute-done | bytes 524320 | tf_op jit(solution)/shard_map/ppermute | solution.py:135
  215.3 2.5 collective-permute-start.2
  217.8 0.4 collective-permute-done.1
  218.2 0.7 collective-permute-start.3
  218.9 5.0 %collective-permute-done.2 = bf16[1024,256]{0,1:T(8,128)(2,1)S(1)} collective-permute-done((bf16[1024,256]{0,1:T(8,128)(2,1)S(1)}, bf16[1024,256]{0,1:T(8,128)(2,1)S(1)}, u32[]{:S(2)}, u32[]{:S(2)}) %collective-permute-start.2) | collective-permute-done | bytes 524320 | tf_op jit(solution)/shard_map/ppermute | solution.py:135
  223.9 2.5 collective-permute-start.4
  226.4 0.1 slice.28
  226.5 0.1 mul.130
  226.6 0.1 slice_bitcast_fusion
  226.6 4.6 %copy.36 = bf16[4,4,1024,128]{3,2,1,0:T(8,128)(2,1)} copy(bf16[4,4,1024,128]{3,2,0,1:T(8,128)(2,1)} %bitcast.61) | data formatting | bytes 8388608 | tf_op jit(solution)/shard_map/transpose | solution.py:48
  231.3 6.4 %copy.37 = bf16[1024,16,128]{0,2,1:T(8,128)(2,1)} copy(bf16[1024,16,128]{2,0,1:T(8,128)(2,1)} %bitcast.59) | data formatting | bytes 8388608 | tf_op jit(solution)/shard_map/transpose | solution.py:16
  237.7 4.8 %copy.35 = bf16[4,4,128,1024]{3,2,1,0:T(8,128)(2,1)} copy(bf16[4,4,128,1024]{3,2,0,1:T(8,128)(2,1)} %bitcast.62) | data formatting | bytes 8388608 | tf_op jit(solution)/shard_map/transpose | solution.py:48
  242.5 2.3 collective-permute-start.5
  244.8 0.9 constant_dynamic-update-slice_fusion.6
  245.7 0.8 constant_dynamic-update-slice_fusion.5
  246.5 0.8 constant_dynamic-update-slice_fusion.4
  247.4 0.9 constant_dynamic-update-slice_fusion.3
  248.2 0.8 constant_dynamic-update-slice_fusion.2
  249.1 2.0 collective-permute-done.5
  251.1 0.8 constant_dynamic-update-slice_fusion.1
  251.9 0.8 constant_dynamic-update-slice_fusion
  252.8 3.1 fusion
  255.9 14.7 %multiply_convert_fusion = bf16[1024,2048]{1,0:T(8,128)(2,1)} fusion(bf16[1024,2048]{0,1:T(8,128)(2,1)} %bitcast.63, f32[2048]{0:T(1024)S(1)} %slice_bitcast_fusion, f32[1024]{0:T(1024)S(1)} %mul.130, bf16[2048,1024]{1,0:T(8,128)(2,1)} %bitcast.64, bf16[1024,2048]{0,1:T(8,128)(2,1)} %constant_dynamic-update-slice_fusion, f32[2048]{0:T(1024)S(1)} %copy-done.8, ...), kind=kOutput, calls=%fused_computation.11 | convolution fusion | flops 8606711808 | bytes 16801792 | tf_op jit(solution)/shard_map/dot_general | solution.py:150
  270.6 2.5 copy.48
  273.0 57.6 %all_to_all.10 = bf16[8,1024,256]{2,1,0:T(8,128)(2,1)S(1)} all-to-all(bf16[8,1024,256]{2,1,0:T(8,128)(2,1)S(1)} %bitcast.60), channel_id=1, replica_groups=mesh['rep'=2,'fs_0'=4,'fs_1'=4,'tp'=8] {'tp'}, dimensions={0} | all-to-all | bytes 8388608 | tf_op jit(solution)/shard_map/all_to_all | solution.py:64
  330.7 0.6 convert_reduce_fusion
  331.2 0.3 copy.40
  331.6 0.1 fusion.79
  331.7 1.0 copy.41
  (53 shorter events, 0.5 us)
Async XLA Ops:
  6.5 197.3 %copy-start = (bf16[4,128,128]{2,1,0:T(8,128)(2,1)S(1)}, bf16[4,128,128]{2,1,0:T(8,128)(2,1)}, u32[]{:S(2)}) copy-start(bf16[4,128,128]{2,1,0:T(8,128)(2,1)} %param.16) | copy-start | bytes 393220
  6.5 80.6 %copy-start.9 = (u32[256]{0:T(256)S(1)}, u32[256]{0:T(256)}, u32[]{:S(2)}) copy-start(u32[256]{0:T(256)} %constant.119) | copy-start | bytes 3076
  6.5 81.8 %copy-start.6 = (f32[4]{0:T(128)S(1)}, f32[4]{0:T(128)}, u32[]{:S(2)}) copy-start(f32[4]{0:T(128)} %param.15) | copy-start | bytes 52
  6.5 81.8 %copy-start.5 = (f32[16]{0:T(128)S(1)}, f32[16]{0:T(128)}, u32[]{:S(2)}) copy-start(f32[16]{0:T(128)} %param.18) | copy-start | bytes 196
  6.5 81.8 %copy-start.4 = (f32[64]{0:T(128)S(1)}, f32[64]{0:T(128)}, u32[]{:S(2)}) copy-start(f32[64]{0:T(128)} %param.21) | copy-start | bytes 772
  6.5 81.8 %copy-start.3 = (f32[128]{0:T(128)S(1)}, f32[128]{0:T(128)}, u32[]{:S(2)}) copy-start(f32[128]{0:T(128)} %param.23) | copy-start | bytes 1540
  6.6 39.2 %all-gather.19.cloned.1.call-start = ((), (), s32[]{:S(2)}) async-start(), calls=%async_computation.5 | async-start | bytes 1310720 | tf_op jit(solution)/shard_map/all_gather | solution.py:45
  8.4 78.6 %all-gather.15.cloned.1.call-start = ((), (), s32[]{:S(2)}) async-start(), calls=%async_computation.3 | async-start | bytes 1310720 | tf_op jit(solution)/shard_map/all_gather | solution.py:45
  10.3 139.8 %all-gather.13.cloned.1.call-start = ((), (), s32[]{:S(2)}) async-start(), calls=%async_computation.2 | async-start | bytes 4718592 | tf_op jit(solution)/shard_map/all_gather | solution.py:107
  11.1 215.6 %all-gather.21.cloned.1.call-start = ((), (), s32[]{:S(2)}) async-start(), calls=%async_computation.6 | async-start | bytes 5242880 | tf_op jit(solution)/shard_map/all_gather | solution.py:45
  45.8 191.9 %all-gather.17.cloned.1.call-start = ((), (), s32[]{:S(2)}) async-start(), calls=%async_computation.4 | async-start | bytes 5242880 | tf_op jit(solution)/shard_map/all_gather | solution.py:45
  86.8 66.7 %copy-start.7 = (f32[2048]{0:T(1024)S(1)}, f32[2048]{0:T(1024)}, u32[]{:S(2)}) copy-start(f32[2048]{0:T(1024)} %param.13) | copy-start | bytes 24580
  150.1 3.5 %copy-start.1 = (bf16[1,1024,2048]{2,1,0:T(8,128)(2,1)S(1)}, bf16[1,1024,2048]{2,1,0:T(8,128)(2,1)}, u32[]{:S(2)}) copy-start(bf16[1,1024,2048]{2,1,0:T(8,128)(2,1)} %all-gather.13.cloned.1.call-done) | copy-start | bytes 12582916
  159.3 29.6 %copy-start.2 = (bf16[1,1024,256]{2,1,0:T(8,128)(2,1)S(1)}, bf16[1,1024,256]{2,1,0:T(8,128)(2,1)}, u32[]{:S(2)}) copy-start(bf16[1,1024,256]{2,1,0:T(8,128)(2,1)} %param.12) | copy-start | bytes 1572868
  161.9 41.9 %all-to-all-start = ((bf16[8,1024,64]{1,2,0:T(8,128)(2,1)}), bf16[8,1024,64]{1,2,0:T(8,128)(2,1)S(1)}, u32[]{:S(2)}, u32[]{:S(2)}) async-start(bf16[8,1024,64]{1,2,0:T(8,128)(2,1)} %broadcast_in_dim.57), calls=%async_computation | async-start | bytes 2097152 | tf_op jit(solution)/shard_map/all_to_all | solution.py:33
  208.1 7.3 %collective-permute-start = (bf16[1024,256]{0,1:T(8,128)(2,1)S(1)}, bf16[1024,256]{0,1:T(8,128)(2,1)S(1)}, u32[]{:S(2)}, u32[]{:S(2)}) collective-permute-start(bf16[1024,256]{0,1:T(8,128)(2,1)S(1)} %get-tuple-element.8), channel_id=1, source_target_pairs={{0,1},{1,2},{2,3},{3,4},{4,5},{5,6},{6,7},{7,0},{8,9},{9,10},{10,1... | collective-permute-start | bytes 1572872 | tf_op jit(solution)/shard_map/ppermute | solution.py:135
  209.2 9.0 %collective-permute-start.1 = (bf16[1024,256]{0,1:T(8,128)(2,1)S(1)}, bf16[1024,256]{0,1:T(8,128)(2,1)S(1)}, u32[]{:S(2)}, u32[]{:S(2)}) collective-permute-start(bf16[1024,256]{0,1:T(8,128)(2,1)S(1)} %get-tuple-element.8), channel_id=1, source_target_pairs={{0,7},{1,0},{2,1},{3,2},{4,3},{5,4},{6,5},{7,6},{8,15},{9,8},{10,9... | collective-permute-start | bytes 1572872 | tf_op jit(solution)/shard_map/ppermute | solution.py:143
  215.3 8.6 %collective-permute-start.2 = (bf16[1024,256]{0,1:T(8,128)(2,1)S(1)}, bf16[1024,256]{0,1:T(8,128)(2,1)S(1)}, u32[]{:S(2)}, u32[]{:S(2)}) collective-permute-start(bf16[1024,256]{0,1:T(8,128)(2,1)S(1)} %collective-permute-done), channel_id=1, source_target_pairs={{0,1},{1,2},{2,3},{3,4},{4,5},{5,6},{6,7},{7,0},{8,9},{9,10},{10,1... | collective-permute-start | bytes 1572872 | tf_op jit(solution)/shard_map/ppermute | solution.py:135
  218.2 24.3 %collective-permute-start.3 = (bf16[1024,256]{0,1:T(8,128)(2,1)S(1)}, bf16[1024,256]{0,1:T(8,128)(2,1)S(1)}, u32[]{:S(2)}, u32[]{:S(2)}) collective-permute-start(bf16[1024,256]{0,1:T(8,128)(2,1)S(1)} %collective-permute-done.1), channel_id=1, source_target_pairs={{0,7},{1,0},{2,1},{3,2},{4,3},{5,4},{6,5},{7,6},{8,15},{9,8},{10,9... | collective-permute-start | bytes 1572872 | tf_op jit(solution)/shard_map/ppermute | solution.py:143
  223.9 21.8 %collective-permute-start.4 = (bf16[1024,256]{0,1:T(8,128)(2,1)S(1)}, bf16[1024,256]{0,1:T(8,128)(2,1)S(1)}, u32[]{:S(2)}, u32[]{:S(2)}) collective-permute-start(bf16[1024,256]{0,1:T(8,128)(2,1)S(1)} %collective-permute-done.2), channel_id=1, source_target_pairs={{0,1},{1,2},{2,3},{3,4},{4,5},{5,6},{6,7},{7,0},{8,9},{9,10},{10,1... | collective-permute-start | bytes 1572872 | tf_op jit(solution)/shard_map/ppermute | solution.py:135
  242.5 8.6 %collective-permute-start.5 = (bf16[1024,256]{0,1:T(8,128)(2,1)S(1)}, bf16[1024,256]{0,1:T(8,128)(2,1)S(1)}, u32[]{:S(2)}, u32[]{:S(2)}) collective-permute-start(bf16[1024,256]{0,1:T(8,128)(2,1)S(1)} %collective-permute-done.3), channel_id=1, source_target_pairs={{0,7},{1,0},{2,1},{3,2},{4,3},{5,4},{6,5},{7,6},{8,15},{9,8},{10,9... | collective-permute-start | bytes 1572872 | tf_op jit(solution)/shard_map/ppermute | solution.py:143
  245.7 6.2 %collective-permute-start.6 = (bf16[1024,256]{0,1:T(8,128)(2,1)S(1)}, bf16[1024,256]{0,1:T(8,128)(2,1)S(1)}, u32[]{:S(2)}, u32[]{:S(2)}) collective-permute-start(bf16[1024,256]{0,1:T(8,128)(2,1)S(1)} %collective-permute-done.4), channel_id=1, source_target_pairs={{0,1},{1,2},{2,3},{3,4},{4,5},{5,6},{6,7},{7,0},{8,9},{9,10},{10,1... | collective-permute-start | bytes 1572872 | tf_op jit(solution)/shard_map/ppermute | solution.py:135
  247.4 8.5 %copy-start.8 = (f32[2048]{0:T(1024)S(1)}, f32[2048]{0:T(1024)}, u32[]{:S(2)}) copy-start(f32[2048]{0:T(1024)} %param.19) | copy-start | bytes 24580
Sparse Core Ops, SparseCore 0:
  9.2 36.5 all-gather.18
  47.6 34.5 all-gather.14
  84.0 38.2 all-gather.12
  124.0 51.7 all-gather.20
  177.4 50.8 all-gather.16
